TPU v7x, 32 devices: a whole 2x2x4 slice. The times are simulated.
32 devices in a mesh: sp: 4 (over z), tp: 8 (over y, x, core).
Axes of the slice: x: 2, y: 2, z: 4, core: 2. Of those that a mesh axis runs over, the one named last changes fastest.
Arguments:
- latent: bfloat16 [3072, 4096], P('sp', 'tp'), may hold values from -600 to 600
- context: bfloat16 [512, 4096], P('sp', 'tp'), may hold values from -600 to 600
- cond: float32 [4096], P('sp'), may hold values from -6 to 6
- ctx_cond: float32 [4096], P('sp'), may hold values from -6 to 6
- w_shift: bfloat16 [4096, 4096], P('sp', 'tp'), may hold values from -0.09375 to 0.09375
- w_scale: bfloat16 [4096, 4096], P('sp', 'tp'), may hold values from -0.09375 to 0.09375
- w_gate: bfloat16 [4096, 4096], P('sp', 'tp'), may hold values from -0.1875 to 0.1875
- norm_gain: float32 [4096], P('tp'), may hold values from 0.1 to 1.9
- w_query: bfloat16 [2048, 4096], P('tp'), may hold values from -0.09375 to 0.09375
- w_key: bfloat16 [2048, 4096], P('tp'), may hold values from -0.09375 to 0.09375
- w_value: bfloat16 [4096, 4096], P('tp'), may hold values from -0.09375 to 0.09375
- w_decay_fwd: bfloat16 [2048, 4096], P('tp'), may hold values from -0.09375 to 0.09375
- w_decay_bwd: bfloat16 [2048, 4096], P('tp'), may hold values from -0.09375 to 0.09375
- forgetting_shift_vector: float32 [2048], P('tp')
- decay_log: float32 [3072, 64], P('sp', 'tp'), may hold values from -3 to 0
- head_gain: float32 [4096], P('tp'), may hold values from 0.1 to 1.9
- w_out: bfloat16 [4096, 4096], P('tp'), may hold values from -0.09375 to 0.09375
Outputs:
- update: bfloat16 [3072, 4096], P('sp', 'tp')
All inputs are finite; a program needn't handle non-finite values.
Results may differ from a plain program's by a relative error of at most 0.012.
The roundings to bfloat16 on the way count: a program that leaves them out, or rounds other values in their place, can miss the bound.
Values may be sent and summed in bfloat16 or wider, within the bound.
A program may use at most 128 MiB of HBM per device.

v0:
```python
import jax
import jax.numpy as jnp
from jax import lax
from jax.sharding import PartitionSpec as P

WIDTH = 4096
ADDRESS_WIDTH = 32
VALUE_DIM = 64
BLOCK = 64


epsilon = 1e-06
smoothing_scale_factor = 16.0
highest_precision = lax.Precision.HIGHEST


def rounded(matrix):
    return lax.optimization_barrier(matrix.astype(jnp.bfloat16)).astype(jnp.float32)


def contract(left, right):
    return lax.dot_general(
        left, right, (((1,), (1,)), ((), ())), preferred_element_type=jnp.float32
    )


def divide_among_attention_units(matrix, head_width):
    return jnp.transpose(matrix.reshape(matrix.shape[0], -1, head_width), (1, 0, 2))


def blockwise(query_rows, key_rows, value_rows, log_decay, initial_state):
    head_count, length, key_width = query_rows.shape
    block_count = length // BLOCK

    def to_blocks(tensor):
        return jnp.moveaxis(tensor.reshape(head_count, block_count, BLOCK, tensor.shape[-1]), 1, 0)

    lower_mask = jnp.tril(jnp.ones((BLOCK, BLOCK), jnp.float32))

    def advance(current_state, inputs):
        query_block, key_block_rows, value_block_rows, decay_block = inputs
        cumulative_logs = jnp.cumsum(decay_block, axis=1)
        block_finish = cumulative_logs[:, -1:, :]
        decayed_query_rows = query_block * jnp.exp(cumulative_logs)
        scores = (
            jnp.einsum(
                "hck,hsk->hcs",
                decayed_query_rows,
                key_block_rows * jnp.exp(-cumulative_logs),
                precision=highest_precision,
            )
            * lower_mask
        )
        output_rows = jnp.einsum(
            "hcs,hsv->hcv", scores, value_block_rows, precision=highest_precision
        )
        output_rows = output_rows + jnp.einsum(
            "sei,siw->sew", decayed_query_rows, current_state, precision=highest_precision
        )
        current_state = jnp.exp(block_finish[:, 0, :])[:, :, None] * current_state + jnp.einsum(
            "zoa,zol->zal",
            key_block_rows * jnp.exp(block_finish - cumulative_logs),
            value_block_rows,
            precision=highest_precision,
        )
        return (current_state, output_rows)

    final_state, outputs = lax.scan(
        advance,
        initial_state,
        (to_blocks(query_rows), to_blocks(key_rows), to_blocks(value_rows), to_blocks(log_decay)),
    )
    return (jnp.moveaxis(outputs, 0, 1).reshape(head_count, length, -1), final_state)


def entering(log_totals, state_rows, place):
    cumulative_logs = jnp.cumsum(log_totals, axis=0)
    before = lax.dynamic_index_in_dim(cumulative_logs, place - 1, 0, keepdims=False)
    position = jnp.arange(log_totals.shape[0])
    exponent_value = jnp.where(
        (position < place)[:, None, None], before[None] - cumulative_logs, -jnp.inf
    )
    return jnp.einsum(
        "aqb,aqbm->qbm", jnp.exp(exponent_value), state_rows, precision=highest_precision
    )


def per_device(
    latent,
    context,
    cond,
    ctx_cond,
    w_shift,
    w_scale,
    w_gate,
    norm_gain,
    w_query,
    w_key,
    w_value,
    w_decay_fwd,
    w_decay_bwd,
    forgetting_shift_vector,
    decay_log,
    head_gain,
    w_out,
):
    tok_rows, channels = latent.shape
    heads_here = forgetting_shift_vector.shape[0] // ADDRESS_WIDTH
    key_columns = heads_here * ADDRESS_WIDTH
    value_columns = heads_here * VALUE_DIM
    activations = jnp.stack([jax.nn.silu(cond), jax.nn.silu(ctx_cond)]).astype(jnp.bfloat16)
    partials = jnp.stack(
        [
            jnp.dot(activations, weight, preferred_element_type=jnp.float32)
            for weight in (w_shift, w_scale, w_gate)
        ],
        axis=1,
    )
    wide_lat = latent.astype(jnp.float32)
    wide_ctx = context.astype(jnp.float32)
    squares_lat = jnp.sum(wide_lat * wide_lat, axis=1)
    squares_ctx = jnp.sum(wide_ctx * wide_ctx, axis=1)
    modulation = lax.psum(partials, "sp")
    total_lat, total_ctx = lax.psum((squares_lat, squares_ctx), "tp")
    shift_full = modulation[:, 0].astype(jnp.bfloat16)
    inverse_lat = lax.rsqrt(total_lat / WIDTH + epsilon)[:, None]
    inverse_ctx = lax.rsqrt(total_ctx / WIDTH + epsilon)[:, None]
    scaled_lat = (wide_lat * (norm_gain * (1.0 + modulation[0, 1]))[None, :]).astype(jnp.bfloat16)
    scaled_ctx = (wide_ctx * (norm_gain * (1.0 + modulation[1, 1]))[None, :]).astype(jnp.bfloat16)
    w_local = jnp.concatenate([w_query, w_key, w_value, w_decay_fwd, w_decay_bwd], axis=0)
    members = (scaled_lat, scaled_ctx, shift_full)
    pieces = (
        lax.all_gather(members[0], "tp", axis=1, tiled=True),
        lax.all_gather(members[1], "tp", axis=1, tiled=True),
        lax.all_gather(members[2], "tp", axis=1, tiled=True),
    )
    w_rows = w_local
    folded = tuple((contract(member, w_rows) for member in pieces))
    main_lat, main_ctx, shift_part = folded
    proj_lat = inverse_lat * main_lat + shift_part[0][None, :]
    proj_ctx = inverse_ctx * main_ctx + shift_part[1][None, :]
    value_end = 2 * key_columns + value_columns
    query_rows = divide_among_attention_units(
        rounded(proj_lat[:, :key_columns]), ADDRESS_WIDTH
    ) * ADDRESS_WIDTH ** (-0.5)
    key_lat = divide_among_attention_units(
        rounded(proj_lat[:, key_columns : 2 * key_columns]), ADDRESS_WIDTH
    )
    value_lat = divide_among_attention_units(
        rounded(proj_lat[:, 2 * key_columns : value_end]), VALUE_DIM
    )
    context_key_rows = divide_among_attention_units(
        rounded(proj_ctx[:, key_columns : 2 * key_columns]), ADDRESS_WIDTH
    )
    context_value_rows = divide_among_attention_units(
        rounded(proj_ctx[:, 2 * key_columns : value_end]), VALUE_DIM
    )
    summand_list = jnp.transpose(decay_log)[:, :, None]

    def log_decays(projected, offset):
        unprocessed_entries = (
            projected[:, offset : offset + key_columns] + forgetting_shift_vector[None, :]
        )
        return divide_among_attention_units(
            jax.nn.log_sigmoid(unprocessed_entries) / smoothing_scale_factor, ADDRESS_WIDTH
        )

    onward_logarithms = log_decays(proj_lat, value_end) + summand_list
    reverse_logarithms = log_decays(proj_lat, value_end + key_columns) + summand_list
    conditioning_onward_logarithms = log_decays(proj_ctx, value_end)
    conditioning_reverse_logarithms = log_decays(proj_ctx, value_end + key_columns)
    zero_state = jnp.zeros((heads_here, ADDRESS_WIDTH, VALUE_DIM), jnp.float32)
    fwd_out, fwd_state = blockwise(query_rows, key_lat, value_lat, onward_logarithms, zero_state)
    flip_queries = jnp.flip(query_rows, 1)
    flip_logb = jnp.flip(reverse_logarithms, 1)
    bwd_out, bwd_state = blockwise(
        flip_queries, jnp.flip(key_lat, 1), jnp.flip(value_lat, 1), flip_logb, zero_state
    )
    fwd_total = jnp.sum(onward_logarithms, axis=1)
    bwd_total = jnp.sum(reverse_logarithms, axis=1)
    cumulative_forward = jnp.cumsum(conditioning_onward_logarithms, axis=1)
    ctx_fwd_state = jnp.einsum(
        "xcq,xcs->xqs",
        context_key_rows * jnp.exp(cumulative_forward[:, -1:, :] - cumulative_forward),
        context_value_rows,
        precision=highest_precision,
    )
    cumulative_backward = jnp.cumsum(conditioning_reverse_logarithms, axis=1)
    ctx_bwd_state = jnp.einsum(
        "xcq,xcs->xqs",
        context_key_rows * jnp.exp(cumulative_backward - conditioning_reverse_logarithms),
        context_value_rows,
        precision=highest_precision,
    )
    ctx_fwd_total = cumulative_forward[:, -1, :]
    ctx_bwd_total = cumulative_backward[:, -1, :]
    log_stack = jnp.stack([fwd_total, bwd_total, ctx_fwd_total, ctx_bwd_total])[None]
    state_stack = jnp.stack([fwd_state, bwd_state, ctx_fwd_state, ctx_bwd_state])[None]
    all_logs, all_states = (
        lax.all_gather(log_stack.astype(jnp.bfloat16), "sp", axis=0, tiled=True).astype(
            log_stack.dtype
        ),
        lax.all_gather(state_stack.astype(jnp.bfloat16), "sp", axis=0, tiled=True).astype(
            state_stack.dtype
        ),
    )
    block_total = all_logs.shape[0]
    block_place = lax.axis_index("sp")
    fwd_logs = jnp.concatenate([all_logs[:, 2], all_logs[:, 0]], axis=0)
    fwd_states = jnp.concatenate([all_states[:, 2], all_states[:, 0]], axis=0)
    bwd_logs = jnp.concatenate([jnp.flip(all_logs[:, 3], 0), jnp.flip(all_logs[:, 1], 0)], axis=0)
    bwd_states = jnp.concatenate(
        [jnp.flip(all_states[:, 3], 0), jnp.flip(all_states[:, 1], 0)], axis=0
    )
    entering_forward = entering(fwd_logs, fwd_states, block_total + block_place)
    enter_bwd = entering(bwd_logs, bwd_states, 2 * block_total - 1 - block_place)
    fwd_mixed = fwd_out + jnp.einsum(
        "dwz,dzn->dwn",
        query_rows * jnp.exp(jnp.cumsum(onward_logarithms, axis=1)),
        entering_forward,
        precision=highest_precision,
    )
    bwd_mixed = bwd_out + jnp.einsum(
        "dwz,dzn->dwn",
        flip_queries * jnp.exp(jnp.cumsum(flip_logb, axis=1)),
        enter_bwd,
        precision=highest_precision,
    )
    mixed = fwd_mixed + jnp.flip(bwd_mixed, 1)
    normed = mixed * lax.rsqrt(jnp.mean(mixed * mixed, axis=2, keepdims=True) + epsilon)
    normed = normed * head_gain.reshape(heads_here, 1, VALUE_DIM)
    head_rows = (
        jnp.transpose(normed, (1, 0, 2)).reshape(tok_rows, value_columns).astype(jnp.bfloat16)
    )
    w_rows = w_out
    projected = contract(lax.all_gather(head_rows, "tp", axis=1, tiled=True), w_rows)
    return (modulation[0, 2][None, :] * projected).astype(jnp.bfloat16)


def solution(mesh):
    return jax.shard_map(
        per_device,
        mesh=mesh,
        in_specs=(
            P("sp", "tp"),
            P("sp", "tp"),
            P("sp"),
            P("sp"),
            P("sp", "tp"),
            P("sp", "tp"),
            P("sp", "tp"),
            P("tp"),
            P("tp", None),
            P("tp", None),
            P("tp", None),
            P("tp", None),
            P("tp", None),
            P("tp"),
            P("sp", "tp"),
            P("tp"),
            P("tp", None),
        ),
        out_specs=P("sp", "tp"),
        check_vma=False,
    )
```

profile of v0, /device:TPU:0, one launch (start us, length us, event | category | flops | bytes accessed | tf_op | source)
XLA Modules:
  0.0 699.2 jit_solution(8635080400127438333)
XLA Ops:
  11.6 20.4 %psum.21 = f32[2,3,512]{2,0,1:T(2,128)S(1)} all-reduce(f32[2,3,512]{2,0,1:T(2,128)S(1)} %pad_maximum_fusion.3), channel_id=1, replica_groups=mesh['sp'=4,'tp'=8] {'sp'}, use_global_device_ids=true, to_apply=%region_0.1 | all-reduce | flops 3072 | bytes 24576 | tf_op jit(solution)/shard_map/psum | solution.py:123
  34.1 12.0 %all-reduce = (f32[768]{0:T(1024)S(1)}, f32[128]{0:T(128)S(1)}) all-reduce(f32[768]{0:T(1024)S(1)} %get-tuple-element.245, f32[128]{0:T(128)S(1)} %get-tuple-element.250), channel_id=1, replica_groups=mesh['sp'=4,'tp'=8] {'tp'}, use_global_device_ids=true, to_apply=%region_2.3 | all-reduce | flops 896 | bytes 7168 | tf_op jit(solution)/shard_map/psum | solution.py:124
  46.1 9.3 %all-gather = bf16[2,1,4096]{2,0,1:T(2,128)(2,1)S(1)} all-gather(bf16[2,1,512]{2,0,1:T(2,128)(2,1)S(1)} %slice.209), channel_id=2, replica_groups=mesh['sp'=4,'tp'=8] {'tp'}, dimensions={2}, use_global_device_ids=true | all-gather | bytes 18432 | tf_op jit(solution)/shard_map/all_gather | solution.py:135
  55.9 1.8 copy-done.7
  61.0 3.3 fusion.74
  66.0 9.2 %fusion.86 = (bf16[128,1536]{1,0:T(8,128)(2,1)S(1)}, f32[128,1536]{1,0:T(8,128)S(1)}) fusion(f32[1536]{0:T(1024)S(1)} %get-tuple-element.189, bf16[128,4096]{1,0:T(8,128)(2,1)} %all-gather.7.cloned.1.call-done, bf16[1536,4096]{1,0:T(8,128)(2,1)} %copy-done.2, f32[128]{0:T(128)S(1)} %add_rsqrt_fusion.2), kind=kOutput, calls=%fused_computation.186 | convolution fusion | flops 1611202560 | bytes 14817792 | tf_op jit(solution)/shard_map/dot_general | solution.py:22
  76.6 23.5 %fusion.89 = f32[8,128,32]{2,0,1:T(8,128)S(1)} fusion(f32[8,128,32]{2,0,1:T(8,128)S(1)} %copy.146), kind=kOutput, calls=%fused_computation.189 | output fusion | flops 4161536 | bytes 262144 | tf_op jit(solution)/shard_map/jit(cumsum)/reduce_window_sum | solution.py:181
  100.1 11.3 %bitcast_multiply_fusion.7 = (f32[8,128,32]{2,0,1:T(8,128)S(1)}, f32[8,128,32]{2,0,1:T(8,128)S(1)}, bf16[8,128,32]{2,0,1:T(8,128)(2,1)S(1)}) fusion(f32[128,8,32]{2,1,0:T(8,128)S(1)} %copy.156, f32[8,128,32]{2,0,1:T(8,128)S(1)} %fusion.89, f32[8,32]{1,0:T(8,128)S(1)} %slice_bitcast_fusion.10, f32[128,8,32]{2,1,0:T(8,128)S(1)} %copy.148), kind=kOutput, calls=%fused_computation.101 | output fusion | flops 4325376 | bytes 721920 | tf_op jit(solution)/shard_map/jit(cumsum)/reduce_window_sum | solution.py:188
  113.8 16.3 %fusion.85 = (bf16[768,1536]{1,0:T(8,128)(2,1)S(1)}, f32[768,1536]{1,0:T(8,128)}) fusion(f32[1536]{0:T(1024)S(1)} %get-tuple-element.190, bf16[768,4096]{1,0:T(8,128)(2,1)} %all-gather.5.cloned.1.call-done, bf16[1536,4096]{1,0:T(8,128)(2,1)} %copy-done.2, f32[768]{0:T(1024)S(1)} %add_rsqrt_fusion.1), kind=kOutput, calls=%fused_computation.185 | convolution fusion | flops 9667215360 | bytes 25961472 | tf_op jit(solution)/shard_map/dot_general | solution.py:22
  131.2 2.5 rev.32
  133.7 1.9 reshape.258
  135.9 2.9 rev.33
  138.8 2.4 reshape.260
  141.2 2.4 fusion.38
  148.6 2.7 reshape.270
  151.3 2.4 reshape.271
  155.7 1.8 reshape.272
  157.5 2.1 broadcast.63.clone
  159.7 181.9 %while.27 = (s32[]{:T(128)}, f32[8,32,64]{2,1,0:T(8,128)S(1)}, f32[12,8,64,64]{3,2,1,0:T(8,128)}, f32[12,8,64,32]{2,0,3,1:T(8,128)}, f32[12,8,64,32]{2,0,3,1:T(8...) while((s32[]{:T(128)}, f32[8,32,64]{2,1,0:T(8,128)S(1)}, ...), condition=%wide.region_17.18_spmd.clone, body=%wide.region_15.17_spmd.clone.sunk | while | flops 64167936 | bytes 3250304 | solution.py:68
  163.3 6.3 fusion.169
  178.5 6.3 fusion.169
  193.6 6.3 fusion.169
  208.8 6.3 fusion.169
  216.2 1.8 constant_dynamic-slice_fusion.17
  223.9 6.3 fusion.169
  239.0 6.3 fusion.169
  254.2 6.3 fusion.169
  269.3 6.3 fusion.169
  284.5 6.3 fusion.169
  299.6 6.3 fusion.169
  314.8 6.3 fusion.169
  330.0 6.3 fusion.169
  341.6 5.2 copy.161
  346.9 4.6 reshape.275
  351.4 13.3 %all_gather.21 = bf16[4,4,8,32]{3,2,1,0:T(8,128)(2,1)S(1)} all-gather(bf16[1,4,8,32]{3,2,1,0:T(8,128)(2,1)S(1)} %pad_maximum_fusion.4), channel_id=1, replica_groups=mesh['sp'=4,'tp'=8] {'sp'}, dimensions={0}, use_global_device_ids=true | all-gather | bytes 10240 | tf_op jit(solution)/shard_map/all_gather | solution.py:200
  366.9 1.9 reshape.256
  368.8 1.8 reshape.262
  370.6 2.1 broadcast.63.clone.1
  372.7 181.7 %while.26 = (s32[]{:T(128)}, f32[8,32,64]{2,1,0:T(8,128)S(1)}, f32[12,8,64,64]{3,2,1,0:T(8,128)}, f32[12,8,64,32]{2,0,3,1:T(8,128)}, f32[12,8,64,32]{2,0,3,1:T(8...) while((s32[]{:T(128)}, f32[8,32,64]{2,1,0:T(8,128)S(1)}, ...), condition=%wide.region_5.6_spmd.clone, body=%wide.region_3.0_spmd.clone.sunk | while | flops 64167936 | bytes 3250304 | solution.py:68
  376.1 6.3 fusion.155
  391.2 6.3 fusion.155
  406.4 6.3 fusion.155
  421.5 6.3 fusion.155
  436.7 6.3 fusion.155
  451.8 6.3 fusion.155
  467.0 6.3 fusion.155
  482.1 6.3 fusion.155
  497.3 6.3 fusion.155
  512.4 6.3 fusion.155
  527.5 6.3 fusion.155
  542.7 6.3 fusion.155
  555.4 19.3 %all_gather.22 = bf16[4,4,8,32,64]{4,3,2,1,0:T(8,128)(2,1)S(1)} all-gather(bf16[1,4,8,32,64]{4,3,2,1,0:T(8,128)(2,1)S(1)} %pad_maximum_fusion.2), channel_id=1, replica_groups=mesh['sp'=4,'tp'=8] {'sp'}, dimensions={0}, use_global_device_ids=true | all-gather | bytes 655360 | tf_op jit(solution)/shard_map/all_gather | solution.py:203
  576.2 1.9 rev.38
  579.0 14.2 %reduce-window.16 = f32[8,32,6,128]{3,1,2,0:T(8,128)S(1)} reduce-window(f32[8,32,6,128]{3,1,2,0:T(8,128)S(1)} %copy-done.8, f32[]{:T(128)} %constant.99.clone.1), window={size=1x1x1x128 pad=0_0x0_0x0_0x127_0}, to_apply=%region_18.19 | reduce-window | flops 24969216 | bytes 1572868 | tf_op jit(solution)/shard_map/reduce-window.2
  595.4 2.3 fusion.33
  597.8 2.9 convolution_add_fusion.4
  600.6 4.9 rev.39
  605.5 5.2 copy.139
  610.8 4.6 reshape.263
  615.7 13.8 %reduce-window.14 = f32[8,32,6,128]{3,1,2,0:T(8,128)S(1)} reduce-window(f32[8,32,6,128]{3,1,2,0:T(8,128)S(1)} %copy_bitcast_fusion.1, f32[]{:T(128)} %constant.99.clone.1), window={size=1x1x1x128 pad=0_0x0_0x0_0x127_0}, to_apply=%region_6.7 | reduce-window | flops 24969216 | bytes 1572868 | tf_op jit(solution)/shard_map/reduce-window
  631.7 2.3 fusion.35
  634.0 3.8 multiply_reduce_fusion
  638.9 45.1 %all-gather.9.cloned.1.call-done = bf16[768,4096]{0,1:T(8,128)(2,1)} async-done(((bf16[768,512]{0,1:T(8,128)(2,1)}), bf16[768,4096]{0,1:T(8,128)(2,1)}) %all-gather.9.cloned.1.call-update) | async-done | bytes 6291472 | tf_op jit(solution)/shard_map/all_gather | solution.py:236
  684.1 8.4 %multiply_convert_fusion = bf16[768,512]{1,0:T(8,128)(2,1)} fusion(bf16[768,4096]{0,1:T(8,128)(2,1)} %all-gather.9.cloned.1.call-done, bf16[512,4096]{1,0:T(8,128)(2,1)} %param.37, f32[512]{0:T(512)S(1)} %bitcast.338), kind=kOutput, calls=%fused_computation.59 | convolution fusion | flops 3222011904 | bytes 11274240 | tf_op jit(solution)/shard_map/dot_general | solution.py:22
  (506 shorter events, 242.7 us)
Async XLA Ops:
  6.5 1.7 copy-start
  6.5 25.5 %copy-start.24 = (f32[512]{0:T(512)S(1)}, f32[512]{0:T(512)}, u32[]{:S(2)}) copy-start(f32[512]{0:T(512)} %param.28) | copy-start | bytes 6148
  6.5 25.5 %copy-start.18 = (bf16[128,512]{1,0:T(8,128)(2,1)S(1)}, bf16[128,512]{1,0:T(8,128)(2,1)}, u32[]{:S(2)}) copy-start(bf16[128,512]{1,0:T(8,128)(2,1)} %param.22) | copy-start | bytes 393220
  6.5 27.5 %copy-start.25 = (f32[512]{0:T(512)S(1)}, f32[512]{0:T(512)}, u32[]{:S(2)}) copy-start(f32[512]{0:T(512)} %param.36) | copy-start | bytes 6148
  6.5 48.9 %copy-start.11 = (bf16[256,4096]{1,0:T(8,128)(2,1)S(1)}, bf16[256,4096]{1,0:T(8,128)(2,1)}, u32[]{:S(2)}) copy-start(bf16[256,4096]{1,0:T(8,128)(2,1)} %param.29) | copy-start | bytes 6291460
  6.5 59.4 %all-gather.7.cloned.1.call-start = ((), (), s32[]{:S(2)}) async-start(), calls=%async_computation.1 | async-start | bytes 1179648 | tf_op jit(solution)/shard_map/all_gather | solution.py:134
  8.5 24.3 %copy-start.17 = (bf16[768,512]{1,0:T(8,128)(2,1)S(1)}, bf16[768,512]{1,0:T(8,128)(2,1)}, u32[]{:S(2)}) copy-start(bf16[768,512]{1,0:T(8,128)(2,1)} %param.21) | copy-start | bytes 2359300
  32.8 81.1 %all-gather.5.cloned.1.call-start = ((), (), s32[]{:S(2)}) async-start(), calls=%async_computation | async-start | bytes 7077888 | tf_op jit(solution)/shard_map/all_gather | solution.py:133
  33.9 650.1 %all-gather.9.cloned.1.call-start = ((), (), s32[]{:S(2)}) async-start(), calls=%async_computation.2 | async-start | bytes 7077888 | tf_op jit(solution)/shard_map/all_gather | solution.py:236
  46.1 9.5 %copy-start.12 = (bf16[256,4096]{1,0:T(8,128)(2,1)S(1)}, bf16[256,4096]{1,0:T(8,128)(2,1)}, u32[]{:S(2)}) copy-start(bf16[256,4096]{1,0:T(8,128)(2,1)} %param.30) | copy-start | bytes 6291460
  55.5 2.2 copy-start.7
  57.7 1.6 copy-start.13
  59.3 1.6 copy-start.14
  61.0 4.9 copy-start.2
  66.0 9.6 %copy-start.23 = (f32[256]{0:T(256)S(1)}, f32[256]{0:T(256)}, u32[]{:S(2)}) copy-start(f32[256]{0:T(256)} %param.34) | copy-start | bytes 3076
  141.2 2.9 copy-start.19
  143.8 2.0 copy-start.3
  145.8 5.5 copy-start.5
  151.3 2.4 copy-start.16
  346.9 20.1 %copy-start.10 = (f32[8,768,32]{1,2,0:T(8,128)S(1)}, f32[8,768,32]{1,2,0:T(8,128)}, u32[]{:S(2)}) copy-start(f32[8,768,32]{1,2,0:T(8,128)} %get-tuple-element.222) | copy-start | bytes 2359300
  351.4 17.4 %copy-start.9 = (f32[8,768,32]{1,2,0:T(8,128)S(1)}, f32[8,768,32]{1,2,0:T(8,128)}, u32[]{:S(2)}) copy-start(f32[8,768,32]{1,2,0:T(8,128)} %broadcast_multiply_fusion.1) | copy-start | bytes 2359300
  575.0 4.0 copy-start.8
  593.8 4.0 copy-start.6
  610.7 4.6 copy-start.21
  610.7 4.6 copy-start.22
  610.7 4.8 copy-start.4
  610.8 4.8 copy-start.20
  615.3 15.2 %copy-start.15 = (f32[4,8,32,64]{3,2,1,0:T(8,128)S(1)}, f32[4,8,32,64]{3,2,1,0:T(8,128)}, u32[]{:S(2)}) copy-start(f32[4,8,32,64]{3,2,1,0:T(8,128)} %get-tuple-element.239) | copy-start | bytes 786436
  684.1 8.4 %copy-start.1 = (bf16[1024,512]{1,0:T(8,128)(2,1)S(1)}, bf16[1024,512]{1,0:T(8,128)(2,1)}, u32[]{:S(2)}) copy-start(bf16[1024,512]{1,0:T(8,128)(2,1)} %param.27) | copy-start | bytes 3145732
Sparse Core Ops, SparseCore 0:
  32.9 21.7 all-gather.6
  56.6 46.5 all-gather.4
  639.1 44.9 all-gather.8
where the time goes:
time: 709 us; the launch traced here: 699 us
  other arithmetic  232 us (33%)
  local copies, waits for them, and re-layouts  202 us (28%)
  matrix products  129 us (18%)
  blocking collectives  74.4 us (10%)
  waiting for transfers between devices  45.2 us (6%)
  between operations  14 us (2%)
    another operation x24, other arithmetic, advance(): cumulative_logs = jnp.cumsum(decay_block, axis=1)  152 us
    dynamic_slice x144, local copies, waits for them, and re-layouts, blockwise(): lax.scan(advance, initial_state, (to_blocks(query_rows), to_blocks(key_ro...  128 us
    all_gather x1, waiting for transfers between devices, per_device(): lax.all_gather(head_rows, 'tp', axis=1, tiled=True)  45.1 us
    dot_general x4, matrix products, contract(): lax.dot_general(left, right, (((1,), (1,)), ((), ())), preferred_element_...  37.3 us
    dot_general x24, matrix products, advance(): jnp.einsum('sei,siw->sew', decayed_query_rows, current_state, precision=h...  32.1 us
    another operation x6, other arithmetic  30.2 us
    another operation x1, other arithmetic, per_device(): cumulative_forward = jnp.cumsum(conditioning_onward_logarithms, axis=1)  23.5 us
    psum x1, blocking collectives, per_device(): modulation = lax.psum(partials, 'sp')  20.4 us
  transfers between devices with their start and end apart: 3, of which 1 were waited for; matrix products, arithmetic and copies ran while one was open for 8% of the time, Pallas kernels for 0%

commit v1 on v0

v1 whole, which is shorter than its diff:
```python
import functools

import jax
import jax.numpy as jnp
from jax import lax
from jax.experimental import pallas as pl
from jax.experimental.pallas import tpu as pltpu
from jax.sharding import PartitionSpec as P

ADDRESS_WIDTH = 32
VALUE_DIM = 64
GROUP = 4
GK = GROUP * ADDRESS_WIDTH
GV = GROUP * VALUE_DIM
PAD = 16
LOG_ROWS = 8

epsilon = 1e-06
smoothing = 16.0
exact = lax.Precision.HIGHEST
F32 = jnp.float32
BF16 = jnp.bfloat16


def block_of(length):
    block = 128
    while length % block:
        block //= 2
    return block


def contract(left, right):
    return lax.dot_general(left, right, (((1,), (1,)), ((), ())), preferred_element_type=F32)


def outer(left, right):
    return lax.dot_general(left, right, (((0,), (0,)), ((), ())), preferred_element_type=F32)


def iota(shape, axis):
    return lax.broadcasted_iota(jnp.int32, shape, axis)


def diagonal_mask():
    return iota((GV, GK), 0) // VALUE_DIM == iota((GV, GK), 1) // ADDRESS_WIDTH


def log_sigmoid(x):
    return jnp.minimum(x, 0.0) - jnp.log1p(jnp.exp(-jnp.abs(x)))


def segment_kernel(
    tok, ctx, main, inv, offset, added, q_out, k_out, v_out, cf_out, cb_out, packet,
    ck, cv, ccf, ccb, kf, kb, ckf, ckb,
):
    kc = q_out.shape[1]
    vc = v_out.shape[1]
    heads = kc // ADDRESS_WIDTH
    ends = (0, kc, 2 * kc, 2 * kc + vc, 3 * kc + vc, 4 * kc + vc)
    expand = (iota((heads, kc), 0) == iota((heads, kc), 1) // ADDRESS_WIDTH).astype(F32)

    def prepare(size, row, shift_row, k_ref, v_ref, cf_ref, cb_ref, at, latent):
        rows = pl.ds(row, size)
        here = pl.ds(at, size)
        scale = inv[rows, :]

        def pre(n):
            cols = pl.ds(ends[n], ends[n + 1] - ends[n])
            return scale * main[rows, cols] + main[pl.ds(shift_row, 1), cols]

        if latent:
            q_out[here, :] = pre(0).astype(BF16)
        k_ref[here, :] = pre(1).astype(BF16)
        v_ref[here, :] = pre(2).astype(BF16)
        log_f = log_sigmoid(pre(3) + offset[...]) / smoothing
        log_b = log_sigmoid(pre(4) + offset[...]) / smoothing
        if latent:
            extra = jnp.dot(added[here, :], expand, precision=exact, preferred_element_type=F32)
            log_f = log_f + extra
            log_b = log_b + extra
        r, c = iota((size, size), 0), iota((size, size), 1)
        lower = (r >= c).astype(F32)
        upper = (r <= c).astype(F32)
        cf_ref[here, :] = jnp.dot(lower, log_f, precision=exact, preferred_element_type=F32)
        cb_ref[here, :] = jnp.dot(upper, log_b, precision=exact, preferred_element_type=F32)

    def segment(length, size, k_ref, v_ref, cf_ref, cb_ref, kf_ref, kb_ref, place):
        count = length // size

        def step(i, totals):
            run_f, run_b = totals
            late = pl.multiple_of((count - 1 - i) * size, size)
            soon = pl.multiple_of(i * size, size)
            cum = cf_ref[pl.ds(late, size), :]
            end = cum[size - 1 :, :]
            kf_ref[pl.ds(late, size), :] = (
                k_ref[pl.ds(late, size), :].astype(F32) * jnp.exp(run_f + end - cum)
            ).astype(BF16)
            cum_b = cb_ref[pl.ds(soon, size), :]
            end_b = cum_b[:1, :]
            kb_ref[pl.ds(soon, size), :] = (
                k_ref[pl.ds(soon, size), :].astype(F32) * jnp.exp(run_b + end_b - cum_b)
            ).astype(BF16)
            return run_f + end, run_b + end_b

        zero = jnp.zeros((1, kc), F32)
        totals = lax.fori_loop(0, count, step, (zero, zero))
        mask = diagonal_mask()
        for way, weighted in enumerate((kf_ref, kb_ref)):
            for g in range(heads // GROUP):
                full = outer(v_ref[:, g * GV : (g + 1) * GV], weighted[:, g * GK : (g + 1) * GK])
                full = jnp.where(mask, full, 0.0)
                state = full[:VALUE_DIM]
                for h in range(1, GROUP):
                    state = state + full[h * VALUE_DIM : (h + 1) * VALUE_DIM]
                packet[place + way, :VALUE_DIM, g * GK : (g + 1) * GK] = state.astype(BF16)
            high = totals[way].astype(BF16).astype(F32)
            low = totals[way] - high
            both = jnp.concatenate(
                [jnp.broadcast_to(high, (LOG_ROWS, kc)), jnp.broadcast_to(low, (LOG_ROWS, kc))], axis=0
            )
            packet[place + way, VALUE_DIM:, :] = both.astype(BF16)

    size = block_of(tok)
    csize = block_of(ctx)

    def latent_step(i, carry):
        at = pl.multiple_of(i * size, size)
        prepare(size, at, tok + ctx, k_out, v_out, cf_out, cb_out, at, True)
        return carry

    lax.fori_loop(0, tok // size, latent_step, 0)
    for i in range(ctx // csize):
        prepare(
            csize, tok + i * csize, tok + ctx + 1, ck, cv, ccf, ccb, i * csize, False
        )
    segment(tok, size, k_out, v_out, cf_out, cb_out, kf, kb, 0)
    segment(ctx, csize, ck, cv, ccf, ccb, ckf, ckb, 2)


def mixer_kernel(segments, q, k, v, cf, cb, packets, gain, out, state_f, state_b, saved):
    tok, kc = q.shape
    groups = kc // GK
    size = block_of(tok)
    count = tok // size
    half = size // 2
    place = lax.axis_index("sp")
    mask = diagonal_mask()

    def entering(way):
        def read(seg, kind):
            part = packets[seg, kind].astype(F32)
            logs = part[VALUE_DIM : VALUE_DIM + 1] + part[VALUE_DIM + LOG_ROWS : VALUE_DIM + LOG_ROWS + 1]
            return jnp.exp(logs), part[:VALUE_DIM]

        order = range(segments) if way == 0 else range(segments - 1, -1, -1)
        state = jnp.zeros((VALUE_DIM, kc), F32)
        for seg in order:
            decay, own = read(seg, 2 + way)
            state = decay * state + own
        for seg in order:
            decay, own = read(seg, way)
            active = seg < place if way == 0 else seg > place
            state = jnp.where(active, decay * state + own, state)
        return state

    for way, ref in ((0, state_f), (1, state_b)):
        state = entering(way)
        for g in range(groups):
            tiled = jnp.concatenate([state[:, g * GK : (g + 1) * GK]] * GROUP, axis=0)
            ref[g] = jnp.where(mask, tiled, 0.0)

    def advance(ref, g, end, cum, k_block, v_block):
        weighted = (k_block * jnp.exp(end - cum)).astype(BF16)
        ref[g] = ref[g] * jnp.exp(end) + jnp.where(mask, outer(v_block, weighted), 0.0)

    def back(i, carry):
        b = count - 1 - i
        rows = pl.ds(pl.multiple_of(b * size, size), size)
        for g in range(groups):
            saved[b, g] = state_b[g].astype(BF16)
            keys = slice(g * GK, (g + 1) * GK)
            cum = cb[rows, keys]
            advance(
                state_b, g, cum[:1], cum, k[rows, keys].astype(F32), v[rows, g * GV : (g + 1) * GV]
            )
        return carry

    lax.fori_loop(0, count, back, 0)

    key_head = iota((size, GK), 1) // ADDRESS_WIDTH
    value_head = iota((size, GV), 1) // VALUE_DIM
    row = iota((size, size), 0)
    col = iota((size, size), 1)
    lower = row >= col
    upper = row <= col
    ones = (iota((GV, GV), 0) // VALUE_DIM == iota((GV, GV), 1) // VALUE_DIM).astype(BF16)

    def ahead(b, carry):
        rows = pl.ds(pl.multiple_of(b * size, size), size)
        for g in range(groups):
            keys = slice(g * GK, (g + 1) * GK)
            q_block = q[rows, keys].astype(F32) * ADDRESS_WIDTH ** (-0.5)
            k_block = k[rows, keys].astype(F32)
            v_block = v[rows, g * GV : (g + 1) * GV]
            cum_f = cf[rows, keys]
            cum_b = cb[rows, keys]
            mid_f = cum_f[half - 1 : half]
            mid_b = cum_b[half : half + 1]
            q_f = (q_block * jnp.exp(cum_f - mid_f)).astype(BF16)
            k_f = (k_block * jnp.exp(mid_f - cum_f)).astype(BF16)
            q_b = (q_block * jnp.exp(cum_b - mid_b)).astype(BF16)
            k_b = (k_block * jnp.exp(mid_b - cum_b)).astype(BF16)
            mixed = contract((q_block * jnp.exp(cum_f)).astype(BF16), state_f[g].astype(BF16))
            mixed = mixed + contract((q_block * jnp.exp(cum_b)).astype(BF16), saved[b, g])
            for h in range(GROUP):
                zero = jnp.zeros_like(q_f)
                s_f = contract(jnp.where(key_head == h, q_f, zero), k_f)
                s_b = contract(jnp.where(key_head == h, q_b, zero), k_b)
                scores = jnp.where(lower, s_f, 0.0) + jnp.where(upper, s_b, 0.0)
                part = jnp.dot(scores.astype(BF16), v_block, preferred_element_type=F32)
                mixed = mixed + jnp.where(value_head == h, part, 0.0)
            advance(state_f, g, cum_f[size - 1 :], cum_f, k_block, v_block)
            square = mixed * mixed
            high = square.astype(BF16)
            low = (square - high.astype(F32)).astype(BF16)
            total = jnp.dot(high, ones, preferred_element_type=F32) + jnp.dot(
                low, ones, preferred_element_type=F32
            )
            normed = mixed * lax.rsqrt(total / VALUE_DIM + epsilon)
            values = slice(g * GV, (g + 1) * GV)
            out[rows, values] = (normed * gain[:, values]).astype(BF16)
        return carry

    lax.fori_loop(0, count, ahead, 0)


LIMIT = 56 * 1024 * 1024


def segments_of(tok, ctx, kc, vc, main, inv, offset, added):
    shape = jax.ShapeDtypeStruct
    return pl.pallas_call(
        functools.partial(segment_kernel, tok, ctx),
        out_shape=(
            shape((tok, kc), BF16),
            shape((tok, kc), BF16),
            shape((tok, vc), BF16),
            shape((tok, kc), F32),
            shape((tok, kc), F32),
            shape((4, VALUE_DIM + 2 * LOG_ROWS, kc), BF16),
        ),
        scratch_shapes=[
            pltpu.VMEM((ctx, kc), BF16),
            pltpu.VMEM((ctx, vc), BF16),
            pltpu.VMEM((ctx, kc), F32),
            pltpu.VMEM((ctx, kc), F32),
            pltpu.VMEM((tok, kc), BF16),
            pltpu.VMEM((tok, kc), BF16),
            pltpu.VMEM((ctx, kc), BF16),
            pltpu.VMEM((ctx, kc), BF16),
        ],
        compiler_params=pltpu.CompilerParams(vmem_limit_bytes=LIMIT),
        name="segments",
    )(main, inv, offset, added)


def mix(q, k, v, cf, cb, packets, gain):
    tok, kc = q.shape
    groups = kc // GK
    return pl.pallas_call(
        functools.partial(mixer_kernel, packets.shape[0]),
        out_shape=jax.ShapeDtypeStruct(v.shape, BF16),
        scratch_shapes=[
            pltpu.VMEM((groups, GV, GK), F32),
            pltpu.VMEM((groups, GV, GK), F32),
            pltpu.VMEM((tok // block_of(tok), groups, GV, GK), BF16),
        ],
        compiler_params=pltpu.CompilerParams(vmem_limit_bytes=LIMIT),
        name="mixer",
    )(q, k, v, cf, cb, packets, gain)


def per_device(
    latent, context, cond, ctx_cond, w_shift, w_scale, w_gate, norm_gain, w_query, w_key, w_value,
    w_decay_fwd, w_decay_bwd, forgetting_shift_vector, decay_log, head_gain, w_out,
):
    tok, ctx = latent.shape[0], context.shape[0]
    kc, vc = w_query.shape[0], w_value.shape[0]
    width = w_query.shape[1]
    rows = lax.all_gather(jnp.concatenate([latent, context], axis=0), "tp", axis=1, tiled=True)
    w_local = jnp.concatenate([w_query, w_key, w_value, w_decay_fwd, w_decay_bwd], axis=0)
    activations = jnp.stack([jax.nn.silu(cond), jax.nn.silu(ctx_cond)]).astype(BF16)
    partials = jnp.concatenate(
        [jnp.dot(activations, w, preferred_element_type=F32) for w in (w_shift, w_scale, w_gate)], axis=0
    )
    modulation = lax.psum(partials, "sp")
    factors = jnp.concatenate([norm_gain[None, :] * (1.0 + modulation[2:4]), modulation[:2]], axis=0)
    factors = lax.all_gather(factors, "tp", axis=1, tiled=True)
    wide = rows.astype(F32)
    inv = lax.rsqrt(jnp.sum(wide * wide, axis=1, keepdims=True) / width + epsilon)
    is_latent = lax.broadcasted_iota(jnp.int32, (tok + ctx, 1), 0) < tok
    scaled = (wide * jnp.where(is_latent, factors[0:1], factors[1:2])).astype(BF16)
    shifts = jnp.pad(factors[2:4].astype(BF16), ((0, PAD - 2), (0, 0)))
    main = contract(jnp.concatenate([scaled, shifts], axis=0), w_local)
    q, k, v, cf, cb, packet = segments_of(
        tok, ctx, kc, vc, main, inv, forgetting_shift_vector[None, :], decay_log
    )
    packets = lax.all_gather(packet, "sp", axis=0, tiled=False)
    head_rows = mix(q, k, v, cf, cb, packets, head_gain[None, :])
    projected = contract(lax.all_gather(head_rows, "tp", axis=1, tiled=True), w_out)
    return (modulation[4:5] * projected).astype(BF16)


def solution(mesh):
    return jax.shard_map(
        per_device,
        mesh=mesh,
        in_specs=(
            P("sp", "tp"), P("sp", "tp"), P("sp"), P("sp"), P("sp", "tp"), P("sp", "tp"), P("sp", "tp"),
            P("tp"), P("tp", None), P("tp", None), P("tp", None), P("tp", None), P("tp", None), P("tp"),
            P("sp", "tp"), P("tp"), P("tp", None),
        ),
        out_specs=P("sp", "tp"),
        check_vma=False,
    )
```

time: 709 us -> 192 us (0.27); the launches traced: 699 us -> 191 us
  other arithmetic: 232 us -> 10.5 us
  local copies, waits for them, and re-layouts: 202 us -> 11.5 us
  matrix products: 129 us -> 27.9 us
  Pallas kernels: 0 us -> 25 us
  blocking collectives: 74.4 us -> 49.6 us
  waiting for transfers between devices: 45.2 us -> 53.2 us
    another operation x38 -> x2, other arithmetic: 218 us -> 1.4 us  [the longest x24 152 us: advance(): cumulative_logs = jnp.cumsum(decay_block, axis=1)]
    dynamic_slice x144 -> x0, local copies, waits for them, and re-layouts: 128 us -> none  [blockwise(): lax.scan(advance, initial_state, (to_blocks(query_rows), to_blocks(key_ro...]
    dot_general x105 -> x3, matrix products: 91.2 us -> 3.18 us  [per_device(): jnp.dot(activations, w, preferred_element_type=F32)]
    reshape x11 -> x0, local copies, waits for them, and re-layouts: 26.1 us -> none  [the longest x8 16.7 us: to_blocks(): tensor.reshape(head_count, block_count, BLOCK, tensor.shape[-1])]
    pallas_call x0 -> x2, Pallas kernels: none -> 25 us  [the longest x1 15.4 us: mix(): pl.pallas_call(functools.partial(mixer_kernel, packets.shape[0]), out_sha...]
    rev x8 -> x0, local copies, waits for them, and re-layouts: 13.7 us -> none  [the longest x1 4.89 us: per_device(): mixed = fwd_mixed + jnp.flip(bwd_mixed, 1)]
    all_gather x3 -> x2, blocking collectives: 41.9 us -> 29 us  [the longest x1 19.7 us: per_device(): packets = lax.all_gather(packet, 'sp', axis=0, tiled=False)]
    dot_general x4 -> x2, matrix products: 37.3 us -> 24.7 us  [contract(): lax.dot_general(left, right, (((1,), (1,)), ((), ())), preferred_element_...]
  transfers between devices with their start and end apart: 3 -> 2, of which waited for: 1 -> 2; matrix products, arithmetic and copies ran while one was open for 8% -> 5% of each run, Pallas kernels for 0% -> 0%
where the time goes in v1:
time: 192 us; the launch traced here: 191 us
  waiting for transfers between devices  53.2 us (28%)
  blocking collectives  49.6 us (26%)
  matrix products  27.9 us (15%)
  Pallas kernels  25 us (13%)
  between operations  13.5 us (7%)
  local copies, waits for them, and re-layouts  11.5 us (6%)
  other arithmetic  10.5 us (5%)
    all_gather x1, waiting for transfers between devices, per_device(): lax.all_gather(head_rows, 'tp', axis=1, tiled=True)  44.5 us
    dot_general x2, matrix products, contract(): lax.dot_general(left, right, (((1,), (1,)), ((), ())), preferred_element_...  24.7 us
    psum x1, blocking collectives, per_device(): modulation = lax.psum(partials, 'sp')  20.5 us
    all_gather x1, blocking collectives, per_device(): packets = lax.all_gather(packet, 'sp', axis=0, tiled=False)  19.7 us
    pallas_call x1, Pallas kernels, mix(): pl.pallas_call(functools.partial(mixer_kernel, packets.shape[0]), out_sha...  15.4 us
    unnamed x19, local copies, waits for them, and re-layouts  10.3 us
    pallas_call x1, Pallas kernels, segments_of(): pl.pallas_call(functools.partial(segment_kernel, tok, ctx), out_shape=(sh...  9.64 us
    all_gather x1, blocking collectives, per_device(): factors = lax.all_gather(factors, 'tp', axis=1, tiled=True)  9.34 us
  transfers between devices with their start and end apart: 2, of which 2 were waited for; matrix products, arithmetic and copies ran while one was open for 5% of the time, Pallas kernels for 0%

profile of v1, /device:TPU:0, one launch (start us, length us, event | category | flops | bytes accessed | tf_op | source)
XLA Modules:
  0.0 191.3 jit_solution(12835076614118882157)
XLA Ops:
  6.5 0.0 copy-start
  6.5 0.0 copy-start.3
  6.5 0.0 all-gather.4.cloned.1.call-start
  6.5 2.4 %pad_maximum_fusion = bf16[896,512]{1,0:T(8,128)(2,1)} fusion(bf16[128,512]{1,0:T(8,128)(2,1)} %param.18, bf16[768,512]{1,0:T(8,128)(2,1)} %param.17), kind=kLoop, calls=%fused_computation.13 | loop fusion | flops 1835008 | bytes 1835008 | tf_op jit(solution)/shard_map/concatenate | solution.py:291
  8.9 0.0 all-gather.4.cloned.1.call-update
  8.9 0.0 all-gather.6.cloned.1.call-start
  9.0 0.7 multiply_convert_fusion.1
  9.7 0.7 multiply_convert_fusion.2
  10.4 0.0 copy-done
  10.4 0.2 fusion.14
  10.6 1.5 fusion.15
  12.1 1.5 fusion.16
  13.6 20.5 %psum.7 = f32[6,512]{1,0:T(8,128)S(1)} all-reduce(f32[6,512]{1,0:T(8,128)S(1)} %pad_maximum_fusion.1), channel_id=1, replica_groups=mesh['sp'=4,'tp'=8] {'sp'}, use_global_device_ids=true, to_apply=%region_0.1 | all-reduce | flops 3072 | bytes 24576 | tf_op jit(solution)/shard_map/psum | solution.py:297
  34.1 0.7 fusion.10
  34.8 9.3 %all_gather.16 = f32[4,4096]{1,0:T(4,128)S(1)} all-gather(f32[4,512]{1,0:T(4,128)S(1)} %pad_maximum_fusion.2), channel_id=1, replica_groups=mesh['sp'=4,'tp'=8] {'tp'}, dimensions={1}, use_global_device_ids=true | all-gather | bytes 73728 | tf_op jit(solution)/shard_map/all_gather | solution.py:299
  44.2 1.7 copy.22.added
  45.8 0.0 copy-start.2
  45.9 0.0 copy-done.3
  45.9 0.0 copy-start.4
  45.9 0.1 constant_dynamic-update-slice_fusion.4
  46.0 0.0 copy-start.5
  46.0 1.9 constant_dynamic-update-slice_fusion.3
  47.9 0.8 copy-done.2
  48.7 0.5 constant_dynamic-update-slice_fusion.2
  49.2 0.2 copy-done.4
  49.4 0.2 constant_dynamic-update-slice_fusion.1
  49.6 0.4 copy-done.5
  50.0 0.2 constant_dynamic-update-slice_fusion
  50.2 0.0 copy-start.6
  50.2 4.5 %copy-done.6 = bf16[1536,4096]{1,0:T(8,128)(2,1)} copy-done((bf16[1536,4096]{1,0:T(8,128)(2,1)}, bf16[1536,4096]{1,0:T(8,128)(2,1)S(1)}, u32[]{:S(2)}) %copy-start.6) | copy-done | bytes 12582936
  54.8 8.6 %all-gather.4.cloned.1.call-done = bf16[896,4096]{1,0:T(8,128)(2,1)} async-done(((bf16[896,512]{1,0:T(8,128)(2,1)}), bf16[896,4096]{1,0:T(8,128)(2,1)}) %all-gather.4.cloned.1.call-update) | async-done | bytes 7340048 | tf_op jit(solution)/shard_map/all_gather | solution.py:291
  63.4 6.0 %fusion.2 = (f32[896]{0:T(1024)S(1)}, bf16[896,4096]{1,0:T(8,128)(2,1)S(1)}) fusion(bf16[896,4096]{1,0:T(8,128)(2,1)} %all-gather.4.cloned.1.call-done, f32[4096]{0:T(1024)S(1)} %bitcast.14, f32[4096]{0:T(1024)S(1)} %bitcast.13, pred[896]{0:T(1024)(128)(4,1)S(1)} %iota_compare_fusion.1), kind=kLoop, calls=%fused_computation.5 | loop fusion | flops 22019200 | bytes 14717312 | tf_op jit(solution)/shard_map/reduce_sum | solution.py:301
  69.4 1.0 rsqrt.7.inv
  70.4 16.3 %fusion.4.main = f32[912,1536]{1,0:T(8,128)} fusion(bf16[1536,4096]{1,0:T(8,128)(2,1)} %copy-done.6, bf16[2,4096]{1,0:T(2,128)(2,1)S(1)} %slice.35, bf16[896,4096]{1,0:T(8,128)(2,1)S(1)} %get-tuple-element.18), kind=kOutput, calls=%fused_computation.7 | convolution fusion | flops 11498029056 | bytes 25542656 | tf_op jit(solution)/shard_map/dot_general | solution.py:33
  86.7 9.6 %segments.1 = (bf16[768,256]{1,0:T(8,128)(2,1)}, bf16[768,256]{1,0:T(8,128)(2,1)}, bf16[768,512]{1,0:T(8,128)(2,1)}, f32[768,256]{1,0:T(8,128)}, f32[768,256]{1,0:T(8,128)}, /*index=5*/bf16[4,80,256]{2,1,0:T(8,128)(2,1)}) custom-call(f32[912,1536]{1,0:T(8,128)} %fusion.4.main, f32[896,1]{1,0:T(8,128)} %rsqrt.7.inv, f32[1,256]{1,0:T(1,128)} %bitcast.17, ...), custom_call_target="tpu_custom_call" | custom-call | tf_op jit(solution)/shard_map/segments/pallas_call | solution.py:243
  96.4 19.7 %all-gather = bf16[16,80,256]{2,1,0:T(8,128)(2,1)} all-gather(bf16[4,80,256]{2,1,0:T(8,128)(2,1)} %get-tuple-element.16), channel_id=2, replica_groups=mesh['sp'=4,'tp'=8] {'sp'}, dimensions={0}, use_global_device_ids=true | all-gather | bytes 819200 | tf_op jit(solution)/shard_map/all_gather | solution.py:309
  116.1 15.4 %mixer.1 = bf16[768,512]{1,0:T(8,128)(2,1)} custom-call(bf16[768,256]{1,0:T(8,128)(2,1)} %get-tuple-element.11.q, bf16[768,256]{1,0:T(8,128)(2,1)} %get-tuple-element.12.k, bf16[768,512]{1,0:T(8,128)(2,1)} %get-tuple-element.13.v, f32[768,256]{1,0:T(8,128)} %get-tuple-element.14.cf, f32[768,256]{1,0:T(8,128)} %get-tuple-element.15.cb, ...), custom_call_target="tpu_custom_call" | custom-call | tf_op jit(solution)/shard_map/mixer/pallas_call | solution.py:271
  131.4 0.0 all-gather.6.cloned.1.call-update
  131.5 44.5 %all-gather.6.cloned.1.call-done = bf16[768,4096]{1,0:T(8,128)(2,1)} async-done(((bf16[768,512]{1,0:T(8,128)(2,1)}), bf16[768,4096]{1,0:T(8,128)(2,1)}) %all-gather.6.cloned.1.call-update) | async-done | bytes 6291472 | tf_op jit(solution)/shard_map/all_gather | solution.py:311
  176.0 0.0 copy-start.1
  176.0 8.4 %multiply_convert_fusion = bf16[768,512]{1,0:T(8,128)(2,1)} fusion(bf16[768,4096]{1,0:T(8,128)(2,1)} %all-gather.6.cloned.1.call-done, bf16[512,4096]{1,0:T(8,128)(2,1)} %param.33, f32[512]{0:T(512)S(1)} %bitcast.16), kind=kOutput, calls=%fused_computation.12 | convolution fusion | flops 3222011904 | bytes 11274240 | tf_op jit(solution)/shard_map/dot_general | solution.py:33
  184.4 0.0 copy-done.1
  (9 shorter events, 0.1 us)
Async XLA Ops:
  6.5 3.9 %copy-start = (bf16[1024,512]{1,0:T(8,128)(2,1)S(1)}, bf16[1024,512]{1,0:T(8,128)(2,1)}, u32[]{:S(2)}) copy-start(bf16[1024,512]{1,0:T(8,128)(2,1)} %param.23) | copy-start | bytes 3145732
  6.5 39.3 %copy-start.3 = (bf16[256,4096]{1,0:T(8,128)(2,1)S(1)}, bf16[256,4096]{1,0:T(8,128)(2,1)}, u32[]{:S(2)}) copy-start(bf16[256,4096]{1,0:T(8,128)(2,1)} %param.25) | copy-start | bytes 6291460
  6.5 56.9 %all-gather.4.cloned.1.call-start = ((), (), s32[]{:S(2)}) async-start(), calls=%async_computation | async-start | bytes 8257536 | tf_op jit(solution)/shard_map/all_gather | solution.py:291
  8.9 167.1 %all-gather.6.cloned.1.call-start = ((), (), s32[]{:S(2)}) async-start(), calls=%async_computation.1 | async-start | bytes 7077888 | tf_op jit(solution)/shard_map/all_gather | solution.py:311
  45.8 2.8 %copy-start.2 = (bf16[512,4096]{1,0:T(8,128)(2,1)S(1)}, bf16[512,4096]{1,0:T(8,128)(2,1)}, u32[]{:S(2)}) copy-start(bf16[512,4096]{1,0:T(8,128)(2,1)} %param.27) | copy-start | bytes 12582916
  45.9 3.5 %copy-start.4 = (bf16[256,4096]{1,0:T(8,128)(2,1)S(1)}, bf16[256,4096]{1,0:T(8,128)(2,1)}, u32[]{:S(2)}) copy-start(bf16[256,4096]{1,0:T(8,128)(2,1)} %param.28) | copy-start | bytes 6291460
  46.0 4.0 %copy-start.5 = (bf16[256,4096]{1,0:T(8,128)(2,1)S(1)}, bf16[256,4096]{1,0:T(8,128)(2,1)}, u32[]{:S(2)}) copy-start(bf16[256,4096]{1,0:T(8,128)(2,1)} %param.29) | copy-start | bytes 6291460
  50.2 4.5 %copy-start.6 = (bf16[1536,4096]{1,0:T(8,128)(2,1)}, bf16[1536,4096]{1,0:T(8,128)(2,1)S(1)}, u32[]{:S(2)}) copy-start(bf16[1536,4096]{1,0:T(8,128)(2,1)S(1)} %constant_dynamic-update-slice_fusion) | copy-start | bytes 37748740
  176.0 8.4 %copy-start.1 = (bf16[1024,512]{1,0:T(8,128)(2,1)S(1)}, bf16[1024,512]{1,0:T(8,128)(2,1)}, u32[]{:S(2)}) copy-start(bf16[1024,512]{1,0:T(8,128)(2,1)} %param.23) | copy-start | bytes 3145732
Sparse Core Ops, SparseCore 0:
  9.2 54.1 all-gather.3
  131.6 44.3 all-gather.5

commit v2 on v1

--- a/solution.py
+++ b/solution.py
@@ -50,7 +50,7 @@
 
 
 def segment_kernel(
-    tok, ctx, main, inv, offset, added, q_out, k_out, v_out, cf_out, cb_out, packet,
+    tok, ctx, main_a, main_b, inv_a, inv_b, offset, added, q_out, k_out, v_out, cf_out, cb_out, packet,
     ck, cv, ccf, ccb, kf, kb, ckf, ckb,
 ):
     kc = q_out.shape[1]
@@ -59,14 +59,14 @@
     ends = (0, kc, 2 * kc, 2 * kc + vc, 3 * kc + vc, 4 * kc + vc)
     expand = (iota((heads, kc), 0) == iota((heads, kc), 1) // ADDRESS_WIDTH).astype(F32)
 
-    def prepare(size, row, shift_row, k_ref, v_ref, cf_ref, cb_ref, at, latent):
+    def prepare(size, main, inv, row, shift_row, k_ref, v_ref, cf_ref, cb_ref, at, latent):
         rows = pl.ds(row, size)
         here = pl.ds(at, size)
         scale = inv[rows, :]
 
         def pre(n):
             cols = pl.ds(ends[n], ends[n + 1] - ends[n])
-            return scale * main[rows, cols] + main[pl.ds(shift_row, 1), cols]
+            return scale * main[rows, cols] + main_b[pl.ds(shift_row, 1), cols]
 
         if latent:
             q_out[here, :] = pre(0).astype(BF16)
@@ -124,21 +124,29 @@
     size = block_of(tok)
     csize = block_of(ctx)
 
-    def latent_step(i, carry):
-        at = pl.multiple_of(i * size, size)
-        prepare(size, at, tok + ctx, k_out, v_out, cf_out, cb_out, at, True)
-        return carry
-
-    lax.fori_loop(0, tok // size, latent_step, 0)
+    first = inv_a.shape[0]
+    shift_row = tok - first + ctx
+
+    def latent_steps(main, inv, start, stop):
+        def step(i, carry):
+            at = pl.multiple_of(i * size, size)
+            row = pl.multiple_of(at - start, size)
+            prepare(size, main, inv, row, shift_row, k_out, v_out, cf_out, cb_out, at, True)
+            return carry
+
+        lax.fori_loop(start // size, stop // size, step, 0)
+
+    latent_steps(main_a, inv_a, 0, first)
+    latent_steps(main_b, inv_b, first, tok)
     for i in range(ctx // csize):
         prepare(
-            csize, tok + i * csize, tok + ctx + 1, ck, cv, ccf, ccb, i * csize, False
+            csize, main_b, inv_b, tok - first + i * csize, shift_row + 1, ck, cv, ccf, ccb, i * csize, False
         )
     segment(tok, size, k_out, v_out, cf_out, cb_out, kf, kb, 0)
     segment(ctx, csize, ck, cv, ccf, ccb, ckf, ckb, 2)
 
 
-def mixer_kernel(segments, q, k, v, cf, cb, packets, gain, out, state_f, state_b, saved):
+def mixer_kernel(segments, first, last, q, k, v, cf, cb, packets, gain, out, state_f, state_b, saved):
     tok, kc = q.shape
     groups = kc // GK
     size = block_of(tok)
@@ -186,7 +194,7 @@
             )
         return carry
 
-    lax.fori_loop(0, count, back, 0)
+    lax.fori_loop(0, count - first, back, 0)
 
     key_head = iota((size, GK), 1) // ADDRESS_WIDTH
     value_head = iota((size, GV), 1) // VALUE_DIM
@@ -196,7 +204,20 @@
     upper = row <= col
     ones = (iota((GV, GV), 0) // VALUE_DIM == iota((GV, GV), 1) // VALUE_DIM).astype(BF16)
 
+    def skip(b, carry):
+        rows = pl.ds(pl.multiple_of(b * size, size), size)
+        for g in range(groups):
+            keys = slice(g * GK, (g + 1) * GK)
+            cum = cf[rows, keys]
+            advance(
+                state_f, g, cum[size - 1 :], cum, k[rows, keys].astype(F32), v[rows, g * GV : (g + 1) * GV]
+            )
+        return carry
+
+    lax.fori_loop(0, first, skip, 0)
+
     def ahead(b, carry):
+        here = pl.ds(pl.multiple_of((b - first) * size, size), size)
         rows = pl.ds(pl.multiple_of(b * size, size), size)
         for g in range(groups):
             keys = slice(g * GK, (g + 1) * GK)
@@ -229,16 +250,16 @@
             )
             normed = mixed * lax.rsqrt(total / VALUE_DIM + epsilon)
             values = slice(g * GV, (g + 1) * GV)
-            out[rows, values] = (normed * gain[:, values]).astype(BF16)
+            out[here, values] = (normed * gain[:, values]).astype(BF16)
         return carry
 
-    lax.fori_loop(0, count, ahead, 0)
+    lax.fori_loop(first, last, ahead, 0)
 
 
 LIMIT = 56 * 1024 * 1024
 
 
-def segments_of(tok, ctx, kc, vc, main, inv, offset, added):
+def segments_of(tok, ctx, kc, vc, *operands):
     shape = jax.ShapeDtypeStruct
     return pl.pallas_call(
         functools.partial(segment_kernel, tok, ctx),
@@ -262,15 +283,15 @@
         ],
         compiler_params=pltpu.CompilerParams(vmem_limit_bytes=LIMIT),
         name="segments",
-    )(main, inv, offset, added)
-
-
-def mix(q, k, v, cf, cb, packets, gain):
+    )(*operands)
+
+
+def mix(first, last, q, k, v, cf, cb, packets, gain):
     tok, kc = q.shape
     groups = kc // GK
     return pl.pallas_call(
-        functools.partial(mixer_kernel, packets.shape[0]),
-        out_shape=jax.ShapeDtypeStruct(v.shape, BF16),
+        functools.partial(mixer_kernel, packets.shape[0], first, last),
+        out_shape=jax.ShapeDtypeStruct(((last - first) * block_of(tok), v.shape[1]), BF16),
         scratch_shapes=[
             pltpu.VMEM((groups, GV, GK), F32),
             pltpu.VMEM((groups, GV, GK), F32),
@@ -281,6 +302,49 @@
     )(q, k, v, cf, cb, packets, gain)
 
 
+def spread_kernel(n, src, dst, send, recv, local):
+    me = lax.axis_index("sp")
+    barrier = pltpu.get_barrier_semaphore()
+    for d in range(1, n):
+        pl.semaphore_signal(
+            barrier, inc=1, device_id={"sp": lax.rem(me + d, n)}, device_id_type=pl.DeviceIdType.MESH
+        )
+    pl.semaphore_wait(barrier, n - 1)
+    copies = [pltpu.make_async_copy(src, dst.at[me], local)]
+    for d in range(1, n):
+        copies.append(
+            pltpu.make_async_remote_copy(
+                src_ref=src,
+                dst_ref=dst.at[me],
+                send_sem=send.at[d - 1],
+                recv_sem=recv.at[d - 1],
+                device_id={"sp": lax.rem(me + d, n)},
+                device_id_type=pl.DeviceIdType.MESH,
+            )
+        )
+    for copy in copies:
+        copy.start()
+    for copy in copies:
+        copy.wait()
+
+
+def spread(packet):
+    n = lax.axis_size("sp")
+    return pl.pallas_call(
+        functools.partial(spread_kernel, n),
+        out_shape=jax.ShapeDtypeStruct((n,) + packet.shape, packet.dtype),
+        in_specs=[pl.BlockSpec(memory_space=pltpu.VMEM)],
+        out_specs=pl.BlockSpec(memory_space=pltpu.VMEM),
+        scratch_shapes=[
+            pltpu.SemaphoreType.DMA((n - 1,)),
+            pltpu.SemaphoreType.DMA((n - 1,)),
+            pltpu.SemaphoreType.DMA,
+        ],
+        compiler_params=pltpu.CompilerParams(collective_id=0, has_side_effects=True),
+        name="spread",
+    )(packet)
+
+
 def per_device(
     latent, context, cond, ctx_cond, w_shift, w_scale, w_gate, norm_gain, w_query, w_key, w_value,
     w_decay_fwd, w_decay_bwd, forgetting_shift_vector, decay_log, head_gain, w_out,
@@ -288,7 +352,13 @@
     tok, ctx = latent.shape[0], context.shape[0]
     kc, vc = w_query.shape[0], w_value.shape[0]
     width = w_query.shape[1]
-    rows = lax.all_gather(jnp.concatenate([latent, context], axis=0), "tp", axis=1, tiled=True)
+    size = block_of(tok)
+    count = tok // size
+    first = count // 2 * size
+    rows_a = lax.all_gather(latent[:first], "tp", axis=1, tiled=True)
+    rows_b = lax.all_gather(
+        jnp.concatenate([latent[first:], context], axis=0), "tp", axis=1, tiled=True
+    )
     w_local = jnp.concatenate([w_query, w_key, w_value, w_decay_fwd, w_decay_bwd], axis=0)
     activations = jnp.stack([jax.nn.silu(cond), jax.nn.silu(ctx_cond)]).astype(BF16)
     partials = jnp.concatenate(
@@ -297,19 +367,29 @@
     modulation = lax.psum(partials, "sp")
     factors = jnp.concatenate([norm_gain[None, :] * (1.0 + modulation[2:4]), modulation[:2]], axis=0)
     factors = lax.all_gather(factors, "tp", axis=1, tiled=True)
-    wide = rows.astype(F32)
-    inv = lax.rsqrt(jnp.sum(wide * wide, axis=1, keepdims=True) / width + epsilon)
-    is_latent = lax.broadcasted_iota(jnp.int32, (tok + ctx, 1), 0) < tok
-    scaled = (wide * jnp.where(is_latent, factors[0:1], factors[1:2])).astype(BF16)
+
+    def inverse(wide):
+        return lax.rsqrt(jnp.sum(wide * wide, axis=1, keepdims=True) / width + epsilon)
+
+    wide_a = rows_a.astype(F32)
+    wide_b = rows_b.astype(F32)
+    is_latent = lax.broadcasted_iota(jnp.int32, (tok - first + ctx, 1), 0) < tok - first
+    scaled_a = (wide_a * factors[0:1]).astype(BF16)
+    scaled_b = (wide_b * jnp.where(is_latent, factors[0:1], factors[1:2])).astype(BF16)
     shifts = jnp.pad(factors[2:4].astype(BF16), ((0, PAD - 2), (0, 0)))
-    main = contract(jnp.concatenate([scaled, shifts], axis=0), w_local)
+    main_a = contract(scaled_a, w_local)
+    main_b = contract(jnp.concatenate([scaled_b, shifts], axis=0), w_local)
     q, k, v, cf, cb, packet = segments_of(
-        tok, ctx, kc, vc, main, inv, forgetting_shift_vector[None, :], decay_log
+        tok, ctx, kc, vc, main_a, main_b, inverse(wide_a), inverse(wide_b),
+        forgetting_shift_vector[None, :], decay_log,
     )
-    packets = lax.all_gather(packet, "sp", axis=0, tiled=False)
-    head_rows = mix(q, k, v, cf, cb, packets, head_gain[None, :])
-    projected = contract(lax.all_gather(head_rows, "tp", axis=1, tiled=True), w_out)
-    return (modulation[4:5] * projected).astype(BF16)
+    packets = spread(packet)
+    parts = []
+    for begin, end in ((0, count // 2), (count // 2, count)):
+        head_rows = mix(begin, end, q, k, v, cf, cb, packets, head_gain[None, :])
+        projected = contract(lax.all_gather(head_rows, "tp", axis=1, tiled=True), w_out)
+        parts.append((modulation[4:5] * projected).astype(BF16))
+    return jnp.concatenate(parts, axis=0)
 
 
 def solution(mesh):

time: 192 us -> 222 us (1.16)
  Pallas kernels: 25 us -> 46.8 us
  blocking collectives: 49.6 us -> 29.9 us
  waiting for transfers between devices: 53.2 us -> 68 us
  matrix products: 27.9 us -> 35.6 us
  local copies, waits for them, and re-layouts: 11.5 us -> 16.2 us
    pallas_call x1 -> x3, Pallas kernels: 15.4 us -> 37.1 us  [the longest x2 19.8 us: mix(): pl.pallas_call(functools.partial(mixer_kernel, packets.shape[0], first, l...]
    all_gather x1 -> x0, blocking collectives: 19.7 us -> none  [per_device(): packets = lax.all_gather(packet, 'sp', axis=0, tiled=False)]
    all_gather x1 -> x2, waiting for transfers between devices: 44.5 us -> 54.8 us  [per_device(): lax.all_gather(head_rows, 'tp', axis=1, tiled=True)]
    dot_general x2 -> x4, matrix products: 24.7 us -> 32.4 us  [contract(): lax.dot_general(left, right, (((1,), (1,)), ((), ())), preferred_element_...]
    all_gather x1 -> x2, waiting for transfers between devices: 8.63 us -> 13.2 us  [the longest x1 13.2 us: per_device(): lax.all_gather(jnp.concatenate([latent[first:], context], axis=0), 'tp',...]
    unnamed x19 -> x21, local copies, waits for them, and re-layouts: 10.3 us -> 12.2 us
    reduce_sum x1 -> x2, other arithmetic: 5.99 us -> 7.45 us  [inverse(): jnp.sum(wide * wide, axis=1, keepdims=True) / width + epsilon]
  transfers between devices with their start and end apart: 2 -> 4, of which waited for: 2 -> 3; matrix products, arithmetic and copies ran while one was open for 5% -> 12% of each run, Pallas kernels for 0% -> 5%
where the time goes in v2:
time: 222 us
  waiting for transfers between devices  68 us (31%)
  Pallas kernels  46.8 us (21%)
  matrix products  35.6 us (16%)
  blocking collectives  29.9 us (13%)
  local copies, waits for them, and re-layouts  16.2 us (7%)
  between operations  13.3 us (6%)
  other arithmetic  11.6 us (5%)
    all_gather x2, waiting for transfers between devices, per_device(): lax.all_gather(head_rows, 'tp', axis=1, tiled=True)  54.8 us
    dot_general x4, matrix products, contract(): lax.dot_general(left, right, (((1,), (1,)), ((), ())), preferred_element_...  32.4 us
    psum x1, blocking collectives, per_device(): modulation = lax.psum(partials, 'sp')  20.5 us
    pallas_call x2, Pallas kernels, mix(): pl.pallas_call(functools.partial(mixer_kernel, packets.shape[0], first, l...  19.8 us
    pallas_call x1, Pallas kernels, spread(): pl.pallas_call(functools.partial(spread_kernel, n), out_shape=jax.ShapeDt...  17.3 us
    all_gather x1, waiting for transfers between devices, per_device(): lax.all_gather(jnp.concatenate([latent[first:], context], axis=0), 'tp',...  13.2 us
    unnamed x21, local copies, waits for them, and re-layouts  12.2 us
    pallas_call x1, Pallas kernels, segments_of(): pl.pallas_call(functools.partial(segment_kernel, tok, ctx), out_shape=(sh...  9.69 us
  transfers between devices with their start and end apart: 4, of which 3 were waited for; matrix products, arithmetic and copies ran while one was open for 12% of the time, Pallas kernels for 5%

profile of v2, /device:TPU:0, one launch (start us, length us, event | category | flops | bytes accessed | tf_op | source)
XLA Modules:
  0.0 221.5 jit_solution(1628430583368217051)
XLA Ops:
  6.5 0.0 copy-start
  6.5 0.0 copy-start.7
  6.5 0.0 copy-start.2
  6.5 0.0 all-gather.5.cloned.1.call-start
  6.5 2.1 fusion.24
  8.6 0.0 all-gather.5.cloned.1.call-update
  8.6 0.0 all-gather.7.cloned.1.call-start
  8.7 1.7 pad_maximum_fusion.1
  10.4 0.0 all-gather.7.cloned.1.call-update
  10.5 0.0 all-gather.11.cloned.1.call-start
  10.5 0.7 multiply_convert_fusion
  11.2 0.7 multiply_convert_fusion.1
  11.9 0.0 copy-done
  11.9 0.2 fusion.21
  12.2 1.5 fusion.22
  13.6 1.5 fusion.23
  15.1 20.5 %psum.7 = f32[6,512]{1,0:T(8,128)S(1)} all-reduce(f32[6,512]{1,0:T(8,128)S(1)} %pad_maximum_fusion.2), channel_id=1, replica_groups=mesh['sp'=4,'tp'=8] {'sp'}, use_global_device_ids=true, to_apply=%region_0.1 | all-reduce | flops 3072 | bytes 24576 | tf_op jit(solution)/shard_map/psum | solution.py:367
  35.7 0.0 copy-done.7
  35.7 9.4 %all_gather.16 = f32[4,4096]{1,0:T(4,128)S(1)} all-gather(f32[4,512]{1,0:T(4,128)S(1)} %pad_maximum_fusion.3), channel_id=1, replica_groups=mesh['sp'=4,'tp'=8] {'tp'}, dimensions={1}, use_global_device_ids=true | all-gather | bytes 73728 | tf_op jit(solution)/shard_map/all_gather | solution.py:369
  45.1 1.7 copy.21.added
  46.8 0.0 copy-start.3
  46.8 0.0 copy-done.2
  46.8 0.0 copy-start.1
  46.8 0.1 constant_dynamic-update-slice_fusion.4
  47.0 1.4 copy-done.3
  48.4 0.1 constant_dynamic-update-slice_fusion.3
  48.5 1.1 copy-done.1
  49.6 0.0 copy-start.4
  49.6 0.5 constant_dynamic-update-slice_fusion.2
  50.1 1.1 copy-done.4
  51.2 0.0 copy-start.5
  51.2 0.2 constant_dynamic-update-slice_fusion.1
  51.4 1.4 copy-done.5
  52.8 0.1 constant_dynamic-update-slice_fusion
  53.0 0.0 copy-start.6
  53.0 4.6 %copy-done.6 = bf16[1536,4096]{1,0:T(8,128)(2,1)} copy-done((bf16[1536,4096]{1,0:T(8,128)(2,1)}, bf16[1536,4096]{1,0:T(8,128)(2,1)S(1)}, u32[]{:S(2)}) %copy-start.6) | copy-done | bytes 12582936
  57.6 0.0 all-gather.5.cloned.1.call-done
  57.6 2.6 %fusion.4 = f32[384]{0:T(512)S(1)} fusion(bf16[384,4096]{1,0:T(8,128)(2,1)} %all-gather.5.cloned.1.call-done), kind=kLoop, calls=%fused_computation.9 | loop fusion | flops 4718208 | bytes 3147264 | tf_op jit(solution)/shard_map/reduce_sum | solution.py:372
  60.2 0.8 rsqrt.14.inv_a
  61.0 10.1 %fusion.11.main_a = f32[384,1536]{1,0:T(8,128)} fusion(bf16[1536,4096]{1,0:T(8,128)(2,1)} %copy-done.6, bf16[384,4096]{1,0:T(8,128)(2,1)} %all-gather.5.cloned.1.call-done, f32[4096]{0:T(1024)S(1)} %bitcast.16), kind=kOutput, calls=%fused_computation.15 | convolution fusion | flops 4836556800 | bytes 18104320 | tf_op jit(solution)/shard_map/dot_general | solution.py:33
  71.1 13.2 %all-gather.7.cloned.1.call-done = bf16[512,4096]{1,0:T(8,128)(2,1)} async-done(((bf16[512,512]{1,0:T(8,128)(2,1)}), bf16[512,4096]{1,0:T(8,128)(2,1)}) %all-gather.7.cloned.1.call-update) | async-done | bytes 4194320 | tf_op jit(solution)/shard_map/all_gather | solution.py:359
  84.2 4.9 %fusion.2 = (f32[512]{0:T(512)S(1)}, bf16[512,4096]{1,0:T(8,128)(2,1)}) fusion(bf16[512,4096]{1,0:T(8,128)(2,1)} %all-gather.7.cloned.1.call-done, f32[4096]{0:T(1024)S(1)} %bitcast.15, f32[4096]{0:T(1024)S(1)} %bitcast.17, pred[512]{0:T(512)(128)(4,1)S(1)} %iota_compare_fusion.1), kind=kLoop, calls=%fused_computation.5 | loop fusion | flops 12582400 | bytes 8423936 | tf_op jit(solution)/shard_map/reduce_sum | solution.py:372
  89.1 0.9 copy.20.inv_b
  90.0 12.4 %fusion.6.main_b = f32[528,1536]{1,0:T(8,128)} fusion(bf16[1536,4096]{1,0:T(8,128)(2,1)} %copy-done.6, bf16[2,4096]{1,0:T(2,128)(2,1)S(1)} %slice.45, bf16[512,4096]{1,0:T(8,128)(2,1)} %get-tuple-element.18), kind=kOutput, calls=%fused_computation.11 | convolution fusion | flops 6656753664 | bytes 20037632 | tf_op jit(solution)/shard_map/dot_general | solution.py:33
  102.4 9.7 %segments.1 = (bf16[768,256]{1,0:T(8,128)(2,1)}, bf16[768,256]{1,0:T(8,128)(2,1)}, bf16[768,512]{1,0:T(8,128)(2,1)}, f32[768,256]{1,0:T(8,128)}, f32[768,256]{1,0:T(8,128)}, /*index=5*/bf16[4,80,256]{2,1,0:T(8,128)(2,1)}) custom-call(f32[384,1536]{1,0:T(8,128)} %fusion.11.main_a, f32[528,1536]{1,0:T(8,128)} %fusion.6.main_b, f32[384,1]{1,0:T(8,128)} %rsqrt.14.inv_a, ...), custom_call_target="tpu_custom_call" | custom-call | tf_op jit(solution)/shard_map/segments/pallas_call | solution.py:264
  112.1 17.3 %spread.1.packets = bf16[4,4,80,256]{3,2,1,0:T(8,128)(2,1)} custom-call(bf16[4,80,256]{2,1,0:T(8,128)(2,1)} %get-tuple-element.16.src), custom_call_target="tpu_custom_call" | custom-call | tf_op jit(solution)/shard_map/spread/pallas_call | solution.py:333
  129.4 9.8 %mixer.3 = bf16[384,512]{1,0:T(8,128)(2,1)} custom-call(bf16[768,256]{1,0:T(8,128)(2,1)} %get-tuple-element.11.q, bf16[768,256]{1,0:T(8,128)(2,1)} %get-tuple-element.12.k, bf16[768,512]{1,0:T(8,128)(2,1)} %get-tuple-element.13.v, f32[768,256]{1,0:T(8,128)} %get-tuple-element.14.cf, f32[768,256]{1,0:T(8,128)} %get-tuple-element.15.cb, ...), custom_call_target="tpu_custom_call" | custom-call | tf_op jit(solution)/shard_map/mixer/pallas_call | solution.py:292
  139.2 0.0 all-gather.11.cloned.1.call-update
  139.2 0.0 all-gather.9.cloned.1.call-start
  139.3 10.0 %mixer.2 = bf16[384,512]{1,0:T(8,128)(2,1)} custom-call(bf16[768,256]{1,0:T(8,128)(2,1)} %get-tuple-element.11.q, bf16[768,256]{1,0:T(8,128)(2,1)} %get-tuple-element.12.k, bf16[768,512]{1,0:T(8,128)(2,1)} %get-tuple-element.13.v, f32[768,256]{1,0:T(8,128)} %get-tuple-element.14.cf, f32[768,256]{1,0:T(8,128)} %get-tuple-element.15.cb, ...), custom_call_target="tpu_custom_call" | custom-call | tf_op jit(solution)/shard_map/mixer/pallas_call | solution.py:292
  149.3 0.0 all-gather.9.cloned.1.call-update
  149.3 25.3 %all-gather.11.cloned.1.call-done = bf16[384,4096]{1,0:T(8,128)(2,1)} async-done(((bf16[384,512]{1,0:T(8,128)(2,1)}), bf16[384,4096]{1,0:T(8,128)(2,1)}) %all-gather.11.cloned.1.call-update) | async-done | bytes 3145744 | tf_op jit(solution)/shard_map/all_gather | solution.py:390
  174.6 5.0 %fusion.16 = bf16[384,512]{1,0:T(8,128)(2,1)S(1)} fusion(bf16[384,4096]{1,0:T(8,128)(2,1)} %all-gather.11.cloned.1.call-done, bf16[512,4096]{1,0:T(8,128)(2,1)} %param.33, f32[512]{0:T(512)S(1)} %bitcast.21), kind=kOutput, calls=%fused_computation.21 | convolution fusion | flops 1611005952 | bytes 7735296 | tf_op jit(solution)/shard_map/dot_general | solution.py:33
  179.6 29.5 %all-gather.9.cloned.1.call-done = bf16[384,4096]{1,0:T(8,128)(2,1)} async-done(((bf16[384,512]{1,0:T(8,128)(2,1)}), bf16[384,4096]{1,0:T(8,128)(2,1)}) %all-gather.9.cloned.1.call-update) | async-done | bytes 3145744 | tf_op jit(solution)/shard_map/all_gather | solution.py:390
  209.1 5.0 %fusion.15 = bf16[384,512]{1,0:T(8,128)(2,1)S(1)} fusion(bf16[384,4096]{1,0:T(8,128)(2,1)} %all-gather.9.cloned.1.call-done, bf16[512,4096]{1,0:T(8,128)(2,1)} %param.33, f32[512]{0:T(512)S(1)} %bitcast.22), kind=kOutput, calls=%fused_computation.20 | convolution fusion | flops 1611005952 | bytes 7735296 | tf_op jit(solution)/shard_map/dot_general | solution.py:33
  214.0 0.9 pad_maximum_fusion
  (11 shorter events, 0.1 us)
Async XLA Ops:
  6.5 5.4 %copy-start = (bf16[1024,512]{1,0:T(8,128)(2,1)S(1)}, bf16[1024,512]{1,0:T(8,128)(2,1)}, u32[]{:S(2)}) copy-start(bf16[1024,512]{1,0:T(8,128)(2,1)} %param.23) | copy-start | bytes 3145732
  6.5 29.1 %copy-start.7 = (f32[512]{0:T(512)S(1)}, f32[512]{0:T(512)}, u32[]{:S(2)}) copy-start(f32[512]{0:T(512)} %param.24) | copy-start | bytes 6148
  6.5 40.3 %copy-start.2 = (bf16[256,4096]{1,0:T(8,128)(2,1)S(1)}, bf16[256,4096]{1,0:T(8,128)(2,1)}, u32[]{:S(2)}) copy-start(bf16[256,4096]{1,0:T(8,128)(2,1)} %param.25) | copy-start | bytes 6291460
  6.5 51.0 %all-gather.5.cloned.1.call-start = ((), (), s32[]{:S(2)}) async-start(), calls=%async_computation | async-start | bytes 3538944 | tf_op jit(solution)/shard_map/all_gather | solution.py:358
  8.6 75.6 %all-gather.7.cloned.1.call-start = ((), (), s32[]{:S(2)}) async-start(), calls=%async_computation.1 | async-start | bytes 4718592 | tf_op jit(solution)/shard_map/all_gather | solution.py:359
  10.5 164.1 %all-gather.11.cloned.1.call-start = ((), (), s32[]{:S(2)}) async-start(), calls=%async_computation.3 | async-start | bytes 3538944 | tf_op jit(solution)/shard_map/all_gather | solution.py:390
  46.8 1.6 copy-start.3
  46.8 2.8 %copy-start.1 = (bf16[512,4096]{1,0:T(8,128)(2,1)S(1)}, bf16[512,4096]{1,0:T(8,128)(2,1)}, u32[]{:S(2)}) copy-start(bf16[512,4096]{1,0:T(8,128)(2,1)} %param.27) | copy-start | bytes 12582916
  49.6 1.6 copy-start.4
  51.2 1.6 copy-start.5
  53.0 4.6 %copy-start.6 = (bf16[1536,4096]{1,0:T(8,128)(2,1)}, bf16[1536,4096]{1,0:T(8,128)(2,1)S(1)}, u32[]{:S(2)}) copy-start(bf16[1536,4096]{1,0:T(8,128)(2,1)S(1)} %constant_dynamic-update-slice_fusion) | copy-start | bytes 37748740
  139.2 69.8 %all-gather.9.cloned.1.call-start = ((), (), s32[]{:S(2)}) async-start(), calls=%async_computation.2 | async-start | bytes 3538944 | tf_op jit(solution)/shard_map/all_gather | solution.py:390
Sparse Core Ops, SparseCore 0:
  9.2 35.5 all-gather.4
  46.7 37.5 all-gather.6
  139.3 35.1 all-gather.10
  176.3 32.7 all-gather.8
